TPU v7x, 32 devices: a whole 2x2x4 slice. The times are simulated.
32 devices in a mesh: rep: 2 (over x), fs: 8 (over z, y), tp: 2 (over core).
Axes of the slice: x: 2, y: 2, z: 4, core: 2. Of those that a mesh axis runs over, the one named last changes fastest.
Arguments:
- inputs: bfloat16 [2, 3072, 2048], P('rep', 'fs', 'tp'), may hold values from -6 to 6
- gate_proj: bfloat16 [2048, 2816], P('fs', 'tp'), may hold values from -0.125 to 0.125
- value_proj: bfloat16 [2048, 2816], P('fs', 'tp'), may hold values from -0.125 to 0.125
- gate_taps: float32 [3, 2816], replicated, may hold values from -3 to 3
- value_taps: float32 [3, 2816], replicated, may hold values from -3 to 3
- out_grad: bfloat16 [2, 3072, 2816], P('rep', 'fs', 'tp'), may hold values from -6 to 6
Outputs:
- in_grad: bfloat16 [2, 3072, 2048], P('rep', 'fs', 'tp')
- gate_proj_grad: float32 [2048, 2816], P('fs', 'tp')
- value_proj_grad: float32 [2048, 2816], P('fs', 'tp')
- gate_taps_grad: float32 [3, 2816], replicated
- value_taps_grad: float32 [3, 2816], replicated
All inputs are finite; a program needn't handle non-finite values.
Results may differ from a plain program's by a relative error of at most 0.013.
Values may be sent and summed in bfloat16 or wider, within the bound.
A program may use at most 128 MiB of HBM per device.

v0:
```python
import jax
import jax.numpy as jnp
from jax import lax
from jax.sharding import PartitionSpec as P

HALO = 8


def shift(x, axis, step):
    count = lax.axis_size(axis)
    return lax.ppermute(x, axis, [(i, (i + step) % count) for i in range(count)])


def with_halo(rows):
    count = lax.axis_size("fs")
    nxt = lax.ppermute(rows[:HALO], "fs", [(i + 1, i) for i in range(count - 1)])
    prv = lax.ppermute(rows[rows.shape[0] - HALO :], "fs", [(i, i + 1) for i in range(count - 1)])
    return jnp.concatenate([rows, nxt, prv], axis=0)


def before(x):
    return jnp.concatenate([x[:, -1:], x[:, :-1]], axis=1)


def after(x):
    return jnp.concatenate([x[:, 1:], x[:, :1]], axis=1)


def shards(inputs, gate_proj, value_proj, gate_taps, value_taps, out_grad):
    contract_cols = (((1,), (1,)), ((), ()))
    contract_rows = (((0,), (0,)), ((), ()))
    reps, fs_count = (lax.axis_size("rep"), lax.axis_size("fs"))
    rep = lax.axis_index("rep")
    tokens, feats = inputs.shape[1:]
    hid = gate_proj.shape[1]
    width = min(hid, -(-hid // reps // 128) * 128)
    last = hid - width

    def start_of(part):
        return jnp.minimum(part * width, last)

    first = start_of(rep)
    dead = rep * width - first
    live = jnp.arange(width) >= dead

    def part_cols(x, part):
        return lax.dynamic_slice_in_dim(x, start_of(part), width, x.ndim - 1)

    w_own = jnp.concatenate(
        [
            jnp.where(live, part_cols(w, rep), jnp.zeros((), w.dtype))
            for w in (gate_proj, value_proj)
        ],
        axis=1,
    )
    w_all = lax.all_gather(w_own, "fs", axis=0, tiled=True)
    x_ext = with_halo(inputs[0])
    g_ext = with_halo(out_grad[0])
    x_blocks, g_blocks = ([x_ext], [part_cols(g_ext, rep)])
    for step in range(1, reps):
        x_blocks.append(shift(x_ext, "rep", step))
        g_blocks.append(shift(part_cols(g_ext, (rep + step) % reps), "rep", step))
    x_all = lax.all_gather(jnp.stack(x_blocks), "tp", axis=2, tiled=True)
    g_all = jnp.stack(g_blocks).astype(jnp.float32)
    ext = tokens + 2 * HALO
    pre = jnp.dot(x_all.reshape(reps * ext, -1), w_all, preferred_element_type=jnp.float32)
    pre = pre.astype(jnp.bfloat16).astype(jnp.float32).reshape(reps, ext, 2 * width)
    tap_start = lax.axis_index("tp") * hid + first
    taps = jnp.concatenate(
        [lax.dynamic_slice_in_dim(t, tap_start, width, 1) for t in (gate_taps, value_taps)], axis=1
    )
    pre_b, pre_a = (before(pre), after(pre))
    mix = taps[0] * pre_b + taps[1] * pre + taps[2] * pre_a
    gate_mix, value_mix = (mix[..., :width], mix[..., width:])
    sig = jax.nn.sigmoid(gate_mix)
    gate_cot = g_all * value_mix * (sig * (1.0 + gate_mix * (1.0 - sig)))
    value_cot = g_all * (gate_mix * sig)
    cot = jnp.concatenate([gate_cot, value_cot], axis=2)
    pre_cot = taps[0] * after(cot) + taps[1] * cot + taps[2] * before(cot)
    pre_cot = pre_cot[:, :tokens].astype(jnp.bfloat16).reshape(reps * tokens, 2 * width)
    tap_terms = jnp.stack(
        [jnp.sum(p[:, :tokens] * cot[:, :tokens], axis=(0, 1)) for p in (pre_b, pre, pre_a)]
    )
    factor = float(tokens * fs_count * reps) ** (-0.5)
    grads = lax.dot_general(
        x_all[:, :tokens].reshape(reps * tokens, -1),
        pre_cot,
        contract_rows,
        preferred_element_type=jnp.float32,
    )
    grads = (grads * factor).astype(jnp.bfloat16)
    own = lax.psum_scatter(grads, "fs", scatter_dimension=0, tiled=True)
    partial_value = lax.dot_general(
        pre_cot, w_all, contract_cols, preferred_element_type=jnp.float32
    )
    partial_value = lax.psum_scatter(
        partial_value.astype(jnp.bfloat16), "tp", scatter_dimension=1, tiled=True
    ).reshape(reps, tokens, feats)
    in_grad = partial_value[0].astype(jnp.float32)
    for step in range(1, reps):
        in_grad += shift(partial_value[step], "rep", -step).astype(jnp.float32)
    blocks = [own]
    for step in range(1, reps):
        blocks.append(shift(own, "rep", step))
    proj_grads = []
    for branch in range(2):
        cols = jnp.zeros((own.shape[0], hid), jnp.bfloat16)
        cut = [b[:, branch * width : (branch + 1) * width] for b in blocks]
        for step in range(reps):
            part = (rep - step) % reps
            place = start_of(part)
            skip = part * width - place
            old = lax.dynamic_slice_in_dim(cols, place, width, 1)
            new = jnp.where(jnp.arange(width) >= skip, cut[step], old)
            cols = lax.dynamic_update_slice_in_dim(cols, new, place, 1)
        proj_grads.append(cols.astype(jnp.float32))
    tap_sum = lax.psum(tap_terms * factor, "fs").reshape(3, 2, width)
    tap_all = lax.all_gather(lax.all_gather(tap_sum, "rep"), "tp")
    halves = []
    for half in range(tap_all.shape[0]):
        cols = [
            tap_all[half, p, :, :, max(0, p * width - last) if p * width > last else 0 :]
            for p in range(reps)
        ]
        halves.append(jnp.concatenate(cols, axis=2))
    taps_out = jnp.concatenate(halves, axis=2)
    return (
        in_grad.astype(jnp.bfloat16)[None],
        proj_grads[0],
        proj_grads[1],
        taps_out[:, 0],
        taps_out[:, 1],
    )


def solution(mesh):
    placed = (P("rep", "fs", "tp"), P("fs", "tp"), P("fs", "tp"), P(), P(), P("rep", "fs", "tp"))
    return jax.shard_map(
        shards,
        mesh=mesh,
        in_specs=placed,
        out_specs=(P("rep", "fs", "tp"), P("fs", "tp"), P("fs", "tp"), P(), P()),
        check_vma=False,
    )
```

profile of v0, /device:TPU:2, one launch (start us, length us, event | category | flops | bytes accessed | tf_op | source)
XLA Modules:
  0.0 368.1 jit_solution(3353467001362223861)
XLA Ops:
  7.2 1.5 copy.18
  8.8 3.4 collective-permute-start.4
  12.3 1.3 collective-permute-start.3
  13.6 9.8 %collective-permute-done.4 = bf16[8,1024]{0,1:T(8,128)(2,1)S(1)} collective-permute-done((bf16[8,1024]{0,1:T(8,128)(2,1)S(1)}, bf16[8,1024]{0,1:T(8,128)(2,1)S(1)}, u32[]{:S(2)}, u32[]{:S(2)}) %collective-permute-start.4) | collective-permute-done | bytes 16416 | tf_op jit(solution)/shard_map/ppermute | solution.py:17
  24.9 16.7 %collective-permute-done.5 = bf16[400,1024]{1,0:T(8,128)(2,1)} collective-permute-done((bf16[400,1024]{1,0:T(8,128)(2,1)S(1)}, bf16[400,1024]{1,0:T(8,128)(2,1)}, u32[]{:S(2)}, u32[]{:S(2)}) %collective-permute-start.5) | collective-permute-done | bytes 819232 | tf_op jit(solution)/shard_map/ppermute | solution.py:11
  41.6 1.4 copy.22
  43.1 1.6 pad_maximum_fusion.4
  44.8 1.5 dynamic-slice_select_fusion.1
  47.3 6.2 %collective-permute-start.1 = (bf16[8,1408]{1,0:T(8,128)(2,1)S(1)}, bf16[8,1408]{1,0:T(8,128)(2,1)S(1)}, u32[]{:S(2)}, u32[]{:S(2)}) collective-permute-start(bf16[8,1408]{1,0:T(8,128)(2,1)S(1)} %get-tuple-element.25), channel_id=1, source_target_pairs={{0,2},{2,4},{4,6},{6,8},{8,10},{10,12},{12,14},{1,3},{3,5},{5,7},{... | collective-permute-start | bytes 67592 | tf_op jit(solution)/shard_map/ppermute | solution.py:17
  53.5 1.5 collective-permute-start
  55.9 4.8 %collective-permute-done = bf16[8,1408]{1,0:T(8,128)(2,1)S(1)} collective-permute-done((bf16[8,1408]{1,0:T(8,128)(2,1)S(1)}, bf16[8,1408]{1,0:T(8,128)(2,1)S(1)}, u32[]{:S(2)}, u32[]{:S(2)}) %collective-permute-start) | collective-permute-done | bytes 22560 | tf_op jit(solution)/shard_map/ppermute | solution.py:16
  60.7 1.6 dynamic-slice_bitcast_fusion
  63.7 4.7 %copy.23 = bf16[2,400,2048]{2,1,0:T(8,128)(2,1)S(1)} copy(bf16[2,400,2048]{1,2,0:T(8,128)(2,1)} %all-gather.4.cloned.1.call-done) | data formatting | bytes 6553600 | tf_op jit(solution)/shard_map/all_gather | solution.py:63
  68.4 97.7 %all-gather.6.cloned.1.call-done = bf16[2048,1536]{1,0:T(8,128)(2,1)} async-done(((bf16[256,1536]{1,0:T(8,128)(2,1)}), bf16[2048,1536]{1,0:T(8,128)(2,1)}) %all-gather.6.cloned.1.call-update) | async-done | bytes 6291472 | tf_op jit(solution)/shard_map/all_gather | solution.py:56
  166.1 8.2 %convolution_convert_fusion = bf16[800,1536]{1,0:T(8,128)(2,1)S(1)} fusion(bf16[800,2048]{1,0:T(8,128)(2,1)S(1)} %bitcast.55, bf16[2048,1536]{1,0:T(8,128)(2,1)} %all-gather.6.cloned.1.call-done), kind=kOutput, calls=%fused_computation.37 | convolution fusion | flops 5034393600 | bytes 12025856 | tf_op jit(solution)/shard_map/dot_general | solution.py:66
  175.0 1.3 fusion.24
  176.3 1.7 fusion.3
  178.0 2.2 convert_multiply_fusion
  181.3 8.2 %fusion.15 = (f32[1536]{0:T(1024)S(1)}, f32[1536]{0:T(1024)S(1)}, f32[1536]{0:T(1024)S(1)}, bf16[2,384,1536]{2,1,0:T(8,128)(2,1)S(1)}) fusion(f32[2,400,1536]{2,1,0:T(8,128)S(1)} %convert.5, f32[2,400,768]{2,1,0:T(8,128)S(1)} %get-tuple-element.11, f32[2,400,768]{2,1,0:T(8,128)S(1)} %get-tuple-element.12, f32[2,399,1536]{2,1,0:T(8,128)S(1)} %get-tuple-element.18, ...), kind=kLoop, calls=%fused_computation.31 | loop fusion | flops 20049408 | bytes 31494144 | tf_op jit(solution)/shard_map/reduce_sum | solution.py:82
  189.6 9.3 %convolution_convert_fusion.1 = bf16[768,2048]{1,0:T(8,128)(2,1)} fusion(bf16[768,1536]{1,0:T(8,128)(2,1)S(1)} %bitcast.56, bf16[2048,1536]{1,0:T(8,128)(2,1)} %all-gather.6.cloned.1.call-done), kind=kOutput, calls=%fused_computation.38 | convolution fusion | flops 4833411072 | bytes 11796480 | tf_op jit(solution)/shard_map/dot_general | solution.py:93
  199.2 8.9 %fusion = bf16[2048,1536]{1,0:T(8,128)(2,1)} fusion(bf16[2,384,1536]{2,1,0:T(8,128)(2,1)S(1)} %get-tuple-element.13, bf16[2,400,2048]{1,2,0:T(8,128)(2,1)} %all-gather.4.cloned.1.call-done), kind=kOutput, calls=%fused_computation.1 | convolution fusion | flops 4838129664 | bytes 11796480 | tf_op jit(solution)/shard_map/dot_general | solution.py:85
  208.3 35.4 %psum.7 = f32[1,3,2,768]{3,2,1,0:T(2,128)S(1)} all-reduce(f32[1,3,2,768]{3,2,1,0:T(2,128)S(1)} %all_gather_reshape.3), channel_id=1, replica_groups=mesh['rep'=2,'fs'=8,'tp'=2] {'fs'}, use_global_device_ids=true, to_apply=%region_5.6 | all-reduce | flops 4608 | bytes 36864 | tf_op jit(solution)/shard_map/psum | solution.py:117
  243.7 4.4 %all_gather.17 = f32[2,3,2,768]{3,2,1,0:T(2,128)S(1)} all-gather(f32[1,3,2,768]{3,2,1,0:T(2,128)S(1)} %psum.7), channel_id=1, replica_groups=mesh['rep'=2,'fs'=8,'tp'=2] {'rep'}, dimensions={0}, use_global_device_ids=true | all-gather | bytes 55296 | tf_op jit(solution)/shard_map/all_gather | solution.py:118
  248.1 1.8 all-gather
  250.0 1.2 slice.184
  252.1 79.1 %reduce-scatter.5.cloned.1.call-done = bf16[256,1536]{1,0:T(8,128)(2,1)} async-done(((bf16[2048,1536]{1,0:T(8,128)(2,1)}), bf16[256,1536]{1,0:T(8,128)(2,1)}) %reduce-scatter.5.cloned.1.call-update) | async-done | bytes 786448 | tf_op jit(solution)/shard_map/reduce_scatter | solution.py:92
  332.4 2.3 fusion.20
  336.0 3.1 dynamic_update_slice.12
  339.2 3.1 dynamic_update_slice.14
  342.3 7.6 %collective-permute-done.7 = bf16[256,1536]{1,0:T(8,128)(2,1)S(1)} collective-permute-done((bf16[256,1536]{1,0:T(8,128)(2,1)}, bf16[256,1536]{1,0:T(8,128)(2,1)S(1)}, u32[]{:S(2)}, u32[]{:S(2)}) %collective-permute-start.7) | collective-permute-done | bytes 786464 | tf_op jit(solution)/shard_map/ppermute | solution.py:11
  350.4 4.4 %dynamic_update_slice.13 = bf16[256,1408]{1,0:T(8,128)(2,1)S(1)} dynamic-update-slice(bf16[256,1408]{1,0:T(8,128)(2,1)S(1)} %dynamic_update_slice.12, bf16[256,768]{1,0:T(8,128)(2,1)S(1)} %get-tuple-element.27, s32[]{:T(128)} %constant.42.clone.1, s32[]{:T(128)S(6)} %select_n.71) | dynamic-update-slice | bytes 786436 | tf_op jit(solution)/shard_map/dynamic_update_slice | solution.py:115
  356.0 4.3 %dynamic_update_slice.15 = bf16[256,1408]{1,0:T(8,128)(2,1)S(1)} dynamic-update-slice(bf16[256,1408]{1,0:T(8,128)(2,1)S(1)} %dynamic_update_slice.14, bf16[256,768]{1,0:T(8,128)(2,1)S(1)} %get-tuple-element.26, s32[]{:T(128)} %constant.42.clone.1, s32[]{:T(128)S(6)} %select_n.71) | dynamic-update-slice | bytes 786436 | tf_op jit(solution)/shard_map/dynamic_update_slice | solution.py:115
  (57 shorter events, 13.4 us)
Async XLA Ops:
  7.2 56.6 %all-gather.4.cloned.1.call-start = ((), (), s32[]{:S(2)}) async-start(), calls=%async_computation.2 | async-start | bytes 6291456 | tf_op jit(solution)/shard_map/all_gather | solution.py:63
  8.8 14.6 %collective-permute-start.4 = (bf16[8,1024]{0,1:T(8,128)(2,1)S(1)}, bf16[8,1024]{0,1:T(8,128)(2,1)S(1)}, u32[]{:S(2)}, u32[]{:S(2)}) collective-permute-start(bf16[8,1024]{0,1:T(8,128)(2,1)S(1)} %get-tuple-element.31), channel_id=1, source_target_pairs={{0,2},{2,4},{4,6},{6,8},{8,10},{10,12},{12,14},{1,3},{3,5},{5,7},{... | collective-permute-start | bytes 49160 | tf_op jit(solution)/shard_map/ppermute | solution.py:17
  12.3 11.2 %collective-permute-start.3 = (bf16[8,1024]{0,1:T(8,128)(2,1)S(1)}, bf16[8,1024]{0,1:T(8,128)(2,1)S(1)}, u32[]{:S(2)}, u32[]{:S(2)}) collective-permute-start(bf16[8,1024]{0,1:T(8,128)(2,1)S(1)} %get-tuple-element.30), channel_id=1, source_target_pairs={{2,0},{4,2},{6,4},{8,6},{10,8},{12,10},{14,12},{3,1},{5,3},{7,5},{... | collective-permute-start | bytes 49160 | tf_op jit(solution)/shard_map/ppermute | solution.py:16
  24.1 17.5 %collective-permute-start.5 = (bf16[400,1024]{1,0:T(8,128)(2,1)S(1)}, bf16[400,1024]{1,0:T(8,128)(2,1)}, u32[]{:S(2)}, u32[]{:S(2)}) collective-permute-start(bf16[400,1024]{1,0:T(8,128)(2,1)S(1)} %copy.21), channel_id=1, source_target_pairs={{0,16},{16,0},{1,17},{17,1},{2,18},{18,2},{3,19},{19,3},{4,20},{20... | collective-permute-start | bytes 2457608 | tf_op jit(solution)/shard_map/ppermute | solution.py:11
  43.1 4.2 %copy-start.1 = (bf16[1,384,1408]{2,1,0:T(8,128)(2,1)S(1)}, bf16[1,384,1408]{2,1,0:T(8,128)(2,1)}, u32[]{:S(2)}) copy-start(bf16[1,384,1408]{2,1,0:T(8,128)(2,1)} %param.11) | copy-start | bytes 3244036
  44.7 121.4 %all-gather.6.cloned.1.call-start = ((), (), s32[]{:S(2)}) async-start(), calls=%async_computation.3 | async-start | bytes 7077888 | tf_op jit(solution)/shard_map/all_gather | solution.py:56
  47.2 202.8 %reduce-scatter.3.cloned.1.call-start = ((), (), s32[]{:S(2)}) async-start(), calls=%async_computation.4 | async-start | bytes 4718592 | tf_op jit(solution)/shard_map/reduce_scatter | solution.py:96
  47.3 8.5 %collective-permute-start.1 = (bf16[8,1408]{1,0:T(8,128)(2,1)S(1)}, bf16[8,1408]{1,0:T(8,128)(2,1)S(1)}, u32[]{:S(2)}, u32[]{:S(2)}) collective-permute-start(bf16[8,1408]{1,0:T(8,128)(2,1)S(1)} %get-tuple-element.25), channel_id=1, source_target_pairs={{0,2},{2,4},{4,6},{6,8},{8,10},{10,12},{12,14},{1,3},{3,5},{5,7},{... | collective-permute-start | bytes 67592 | tf_op jit(solution)/shard_map/ppermute | solution.py:17
  53.5 7.1 %collective-permute-start = (bf16[8,1408]{1,0:T(8,128)(2,1)S(1)}, bf16[8,1408]{1,0:T(8,128)(2,1)S(1)}, u32[]{:S(2)}, u32[]{:S(2)}) collective-permute-start(bf16[8,1408]{1,0:T(8,128)(2,1)S(1)} %get-tuple-element.24), channel_id=1, source_target_pairs={{2,0},{4,2},{6,4},{8,6},{10,8},{12,10},{14,12},{3,1},{5,3},{7,5},{... | collective-permute-start | bytes 67592 | tf_op jit(solution)/shard_map/ppermute | solution.py:16
  62.3 115.7 %collective-permute-start.2 = (bf16[400,768]{1,0:T(8,128)(2,1)}, bf16[400,768]{1,0:T(8,128)(2,1)}, u32[]{:S(2)}, u32[]{:S(2)}) collective-permute-start(bf16[400,768]{1,0:T(8,128)(2,1)} %get-tuple-element.23), channel_id=1, source_target_pairs={{0,16},{16,0},{1,17},{17,1},{2,18},{18,2},{3,19},{19,3},{4,20},{20... | collective-permute-start | bytes 1843208 | tf_op jit(solution)/shard_map/ppermute | solution.py:11
  176.3 1.7 copy-start
  198.9 132.3 %reduce-scatter.5.cloned.1.call-start = ((), (), s32[]{:S(2)}) async-start(), calls=%async_computation.5 | async-start | bytes 7077888 | tf_op jit(solution)/shard_map/reduce_scatter | solution.py:92
  251.3 81.2 %collective-permute-start.6 = (bf16[384,1024]{1,0:T(8,128)(2,1)S(1)}, bf16[384,1024]{1,0:T(8,128)(2,1)S(1)}, u32[]{:S(2)}, u32[]{:S(2)}) collective-permute-start(bf16[384,1024]{1,0:T(8,128)(2,1)S(1)} %slice.184), channel_id=1, source_target_pairs={{0,16},{16,0},{1,17},{17,1},{2,18},{18,2},{3,19},{19,3},{4,20},{20... | collective-permute-start | bytes 2359304 | tf_op jit(solution)/shard_map/ppermute | solution.py:11
  331.2 18.7 %collective-permute-start.7 = (bf16[256,1536]{1,0:T(8,128)(2,1)}, bf16[256,1536]{1,0:T(8,128)(2,1)S(1)}, u32[]{:S(2)}, u32[]{:S(2)}) collective-permute-start(bf16[256,1536]{1,0:T(8,128)(2,1)} %reduce-scatter.5.cloned.1.call-done), channel_id=1, source_target_pairs={{0,16},{16,0},{1,17},{17,1},{2,18},{18,2},{3,19},{19,3},{4,20},{20... | collective-permute-start | bytes 2359304 | tf_op jit(solution)/shard_map/ppermute | solution.py:11
Sparse Core Ops, SparseCore 0:
  44.8 18.8 all-gather.3
  66.5 99.5 all-gather.5
  199.0 9.4 reduce-scatter.2
  212.0 119.1 reduce-scatter.4
where the time goes:
time: 369 us; the launch traced here: 368 us
  waiting for transfers between devices  217 us (59%)
  blocking collectives  41.6 us (11%)
  local copies, waits for them, and re-layouts  29 us (8%)
  matrix products  26.4 us (7%)
  other arithmetic  24.7 us (7%)
  starting transfers between devices  15.3 us (4%)
  between operations  14.2 us (4%)
    all_gather x1, waiting for transfers between devices, shards(): w_all = lax.all_gather(w_own, 'fs', axis=0, tiled=True)  97.7 us
    reduce_scatter x1, waiting for transfers between devices, shards(): own = lax.psum_scatter(grads, 'fs', scatter_dimension=0, tiled=True)  79.1 us
    psum x1, blocking collectives, shards(): tap_sum = lax.psum(tap_terms * factor, 'fs').reshape(3, 2, width)  35.4 us
    ppermute x4, waiting for transfers between devices, shift(): lax.ppermute(x, axis, [(i, (i + step) % count) for i in range(count)])  24.4 us
    dynamic_update_slice x4, local copies, waits for them, and re-layouts, shards(): cols = lax.dynamic_update_slice_in_dim(cols, new, place, 1)  15 us
    ppermute x2, waiting for transfers between devices, with_halo(): lax.ppermute(rows[rows.shape[0] - HALO:], 'fs', [(i, i + 1) for i in rang...  9.85 us
    ppermute x2, starting transfers between devices, with_halo(): lax.ppermute(rows[rows.shape[0] - HALO:], 'fs', [(i, i + 1) for i in rang...  9.6 us
    dot_general x1, matrix products, shards(): lax.dot_general(pre_cot, w_all, contract_cols, preferred_element_type=jnp...  9.31 us
  transfers between devices with their start and end apart: 12, of which 7 were waited for; matrix products, arithmetic and copies ran while one was open for 12% of the time, Pallas kernels for 0%

commit v1 on v0

--- a/solution.py
+++ b/solution.py
@@ -53,7 +53,12 @@
         ],
         axis=1,
     )
-    w_all = lax.all_gather(w_own, "fs", axis=0, tiled=True)
+    ring = [w_own]
+    for hop in range(7):
+        ring.append(lax.ppermute(ring[-1], "fs", [(dev, (dev + 1) % 8) for dev in range(8)]))
+    w_all = jnp.roll(
+        jnp.concatenate(ring[::-1], axis=0), (lax.axis_index("fs") + 1) * ring[0].shape[0], axis=0
+    )
     x_ext = with_halo(inputs[0])
     g_ext = with_halo(out_grad[0])
     x_blocks, g_blocks = ([x_ext], [part_cols(g_ext, rep)])

time: 369 us -> 379 us (1.027)
  local copies, waits for them, and re-layouts: 29 us -> 40.6 us
  starting transfers between devices: 15.3 us -> 19.3 us
  waiting for transfers between devices: 217 us -> 213 us
    all_gather x1 -> x0, waiting for transfers between devices: 97.7 us -> none  [shards(): w_all = lax.all_gather(w_own, 'fs', axis=0, tiled=True)]
    ppermute x0 -> x7, waiting for transfers between devices: none -> 77.9 us  [shards(): lax.ppermute(ring[-1], 'fs', [(dev, (dev + 1) % 8) for dev in range(8)])]
    ppermute x2, waiting for transfers between devices: 9.85 us -> 28.2 us  [with_halo(): lax.ppermute(rows[rows.shape[0] - HALO:], 'fs', [(i, i + 1) for i in rang...]
    unnamed x9 -> x31, local copies, waits for them, and re-layouts: 1.53 us -> 10.3 us
    ppermute x0 -> x7, starting transfers between devices: none -> 5.05 us  [shards(): lax.ppermute(ring[-1], 'fs', [(dev, (dev + 1) % 8) for dev in range(8)])]
  transfers between devices with their start and end apart: 12 -> 18, of which waited for: 7 -> 11; matrix products, arithmetic and copies ran while one was open for 12% -> 15% of each run, Pallas kernels for 0% -> 0%
where the time goes in v1:
time: 379 us; the launch traced here: 378 us
  waiting for transfers between devices  213 us (56%)
  local copies, waits for them, and re-layouts  40.6 us (11%)
  blocking collectives  40.4 us (11%)
  other arithmetic  27.2 us (7%)
  matrix products  23.6 us (6%)
  starting transfers between devices  19.3 us (5%)
  between operations  14.3 us (4%)
    reduce_scatter x1, waiting for transfers between devices, shards(): own = lax.psum_scatter(grads, 'fs', scatter_dimension=0, tiled=True)  79.2 us
    ppermute x7, waiting for transfers between devices, shards(): lax.ppermute(ring[-1], 'fs', [(dev, (dev + 1) % 8) for dev in range(8)])  77.9 us
    psum x1, blocking collectives, shards(): tap_sum = lax.psum(tap_terms * factor, 'fs').reshape(3, 2, width)  34.2 us
    ppermute x2, waiting for transfers between devices, with_halo(): lax.ppermute(rows[rows.shape[0] - HALO:], 'fs', [(i, i + 1) for i in rang...  28.2 us
    ppermute x4, waiting for transfers between devices, shift(): lax.ppermute(x, axis, [(i, (i + step) % count) for i in range(count)])  22.8 us
    dynamic_update_slice x4, local copies, waits for them, and re-layouts, shards(): cols = lax.dynamic_update_slice_in_dim(cols, new, place, 1)  15 us
    unnamed x31, local copies, waits for them, and re-layouts  10.3 us
    dot_general x1, matrix products, shards(): lax.dot_general(pre_cot, w_all, contract_cols, preferred_element_type=jnp...  9.22 us
  transfers between devices with their start and end apart: 18, of which 11 were waited for; matrix products, arithmetic and copies ran while one was open for 15% of the time, Pallas kernels for 0%

profile of v1, /device:TPU:2, one launch (start us, length us, event | category | flops | bytes accessed | tf_op | source)
XLA Modules:
  0.0 378.1 jit_solution(14543180809324768747)
XLA Ops:
  8.8 1.6 collective-permute-start.6
  10.4 20.6 %collective-permute-done.6 = bf16[256,1536]{1,0:T(8,128)(2,1)S(1)} collective-permute-done((bf16[256,1536]{1,0:T(8,128)(2,1)S(1)}, bf16[256,1536]{1,0:T(8,128)(2,1)S(1)}, u32[]{:S(2)}, u32[]{:S(2)}) %collective-permute-start.6) | collective-permute-done | bytes 786464 | tf_op jit(solution)/shard_map/ppermute | solution.py:58
  31.0 1.8 copy.18
  32.9 3.5 collective-permute-start.4
  37.6 20.9 %collective-permute-done.4 = bf16[8,1024]{0,1:T(8,128)(2,1)} collective-permute-done((bf16[8,1024]{0,1:T(8,128)(2,1)S(1)}, bf16[8,1024]{0,1:T(8,128)(2,1)}, u32[]{:S(2)}, u32[]{:S(2)}) %collective-permute-start.4) | collective-permute-done | bytes 16416 | tf_op jit(solution)/shard_map/ppermute | solution.py:17
  62.3 2.6 collective-permute-start.8
  66.1 15.2 %collective-permute-done.5 = bf16[400,1024]{1,0:T(8,128)(2,1)} collective-permute-done((bf16[400,1024]{1,0:T(8,128)(2,1)}, bf16[400,1024]{1,0:T(8,128)(2,1)}, u32[]{:S(2)}, u32[]{:S(2)}) %collective-permute-start.5) | collective-permute-done | bytes 819232 | tf_op jit(solution)/shard_map/ppermute | solution.py:11
  84.7 1.6 pad_maximum_fusion.4
  86.4 18.1 %collective-permute-done.9 = bf16[256,1536]{1,0:T(8,128)(2,1)} collective-permute-done((bf16[256,1536]{1,0:T(8,128)(2,1)}, bf16[256,1536]{1,0:T(8,128)(2,1)}, u32[]{:S(2)}, u32[]{:S(2)}) %collective-permute-start.9) | collective-permute-done | bytes 786464 | tf_op jit(solution)/shard_map/ppermute | solution.py:58
  104.4 19.6 %collective-permute-done.10 = bf16[256,1536]{1,0:T(8,128)(2,1)S(1)} collective-permute-done((bf16[256,1536]{1,0:T(8,128)(2,1)}, bf16[256,1536]{1,0:T(8,128)(2,1)S(1)}, u32[]{:S(2)}, u32[]{:S(2)}) %collective-permute-start.10) | collective-permute-done | bytes 786464 | tf_op jit(solution)/shard_map/ppermute | solution.py:58
  124.1 18.6 %collective-permute-done.11 = bf16[256,1536]{1,0:T(8,128)(2,1)S(1)} collective-permute-done((bf16[256,1536]{1,0:T(8,128)(2,1)S(1)}, bf16[256,1536]{1,0:T(8,128)(2,1)S(1)}, u32[]{:S(2)}, u32[]{:S(2)}) %collective-permute-start.11) | collective-permute-done | bytes 786464 | tf_op jit(solution)/shard_map/ppermute | solution.py:58
  143.4 3.4 collective-permute-start.1
  149.2 7.3 %collective-permute-done.1 = bf16[8,1408]{1,0:T(8,128)(2,1)S(1)} collective-permute-done((bf16[8,1408]{1,0:T(8,128)(2,1)S(1)}, bf16[8,1408]{1,0:T(8,128)(2,1)S(1)}, u32[]{:S(2)}, u32[]{:S(2)}) %collective-permute-start.1) | collective-permute-done | bytes 22560 | tf_op jit(solution)/shard_map/ppermute | solution.py:17
  156.5 4.4 %collective-permute-done = bf16[8,1408]{1,0:T(8,128)(2,1)S(1)} collective-permute-done((bf16[8,1408]{1,0:T(8,128)(2,1)S(1)}, bf16[8,1408]{1,0:T(8,128)(2,1)S(1)}, u32[]{:S(2)}, u32[]{:S(2)}) %collective-permute-start) | collective-permute-done | bytes 22560 | tf_op jit(solution)/shard_map/ppermute | solution.py:16
  165.1 6.1 %copy.23 = bf16[2,400,2048]{2,1,0:T(8,128)(2,1)} copy(bf16[2,400,2048]{1,2,0:T(8,128)(2,1)} %all-gather.3.cloned.1.call-done) | data formatting | bytes 6553600 | tf_op jit(solution)/shard_map/all_gather | solution.py:68
  179.1 5.5 %fusion.22 = bf16[800,1536]{1,0:T(8,128)(2,1)S(1)} fusion(bf16[800,2048]{1,0:T(8,128)(2,1)S(1)} %bitcast.53, bf16[4096,1536]{1,0:T(8,128)(2,1)S(1)} %constant_dynamic-update-slice_fusion, s32[]{:T(128)S(6)} %select_n.80), kind=kOutput, calls=%fused_computation.41 | convolution fusion | flops 5034393600 | bytes 12025860 | tf_op jit(solution)/shard_map/dot_general | solution.py:71
  186.6 1.7 fusion.7
  188.3 2.2 convert_multiply_fusion
  191.6 8.2 %fusion.19 = (f32[1536]{0:T(1024)S(1)}, f32[1536]{0:T(1024)S(1)}, f32[1536]{0:T(1024)S(1)}, bf16[2,384,1536]{2,1,0:T(8,128)(2,1)S(1)}) fusion(f32[2,400,1536]{2,1,0:T(8,128)S(1)} %convert.5, f32[2,400,768]{2,1,0:T(8,128)S(1)} %get-tuple-element.11, f32[2,400,768]{2,1,0:T(8,128)S(1)} %get-tuple-element.12, f32[2,399,1536]{2,1,0:T(8,128)S(1)} %get-tuple-element.18, ...), kind=kLoop, calls=%fused_computation.35 | loop fusion | flops 20049408 | bytes 31494144 | tf_op jit(solution)/shard_map/reduce_sum | solution.py:87
  199.9 9.2 %fusion.25 = bf16[768,2048]{1,0:T(8,128)(2,1)} fusion(bf16[768,1536]{1,0:T(8,128)(2,1)S(1)} %bitcast.54, bf16[4096,1536]{1,0:T(8,128)(2,1)} %copy-done.5, s32[]{:T(128)S(6)} %select_n.80), kind=kOutput, calls=%fused_computation.42 | convolution fusion | flops 4833411072 | bytes 11796484 | tf_op jit(solution)/shard_map/dot_general | solution.py:98
  209.4 8.9 %fusion = bf16[2048,1536]{1,0:T(8,128)(2,1)} fusion(bf16[2,384,1536]{2,1,0:T(8,128)(2,1)S(1)} %get-tuple-element.13, bf16[2,400,2048]{1,2,0:T(8,128)(2,1)} %all-gather.3.cloned.1.call-done), kind=kOutput, calls=%fused_computation.1 | convolution fusion | flops 4838129664 | bytes 11796480 | tf_op jit(solution)/shard_map/dot_general | solution.py:90
  218.5 34.2 %psum.7 = f32[1,3,2,768]{3,2,1,0:T(2,128)S(1)} all-reduce(f32[1,3,2,768]{3,2,1,0:T(2,128)S(1)} %all_gather_reshape.3), channel_id=1, replica_groups=mesh['rep'=2,'fs'=8,'tp'=2] {'fs'}, use_global_device_ids=true, to_apply=%region_5.6 | all-reduce | flops 4608 | bytes 36864 | tf_op jit(solution)/shard_map/psum | solution.py:122
  252.7 4.4 %all_gather.13 = f32[2,3,2,768]{3,2,1,0:T(2,128)S(1)} all-gather(f32[1,3,2,768]{3,2,1,0:T(2,128)S(1)} %psum.7), channel_id=1, replica_groups=mesh['rep'=2,'fs'=8,'tp'=2] {'rep'}, dimensions={0}, use_global_device_ids=true | all-gather | bytes 55296 | tf_op jit(solution)/shard_map/all_gather | solution.py:123
  257.1 1.8 all-gather
  260.2 1.7 collective-permute-start.13
  262.0 79.2 %reduce-scatter.5.cloned.1.call-done = bf16[256,1536]{1,0:T(8,128)(2,1)} async-done(((bf16[2048,1536]{1,0:T(8,128)(2,1)}), bf16[256,1536]{1,0:T(8,128)(2,1)}) %reduce-scatter.5.cloned.1.call-update) | async-done | bytes 786448 | tf_op jit(solution)/shard_map/reduce_scatter | solution.py:97
  342.4 2.3 fusion.30
  346.0 3.1 dynamic_update_slice.12
  349.2 3.1 dynamic_update_slice.14
  352.3 7.6 %collective-permute-done.14 = bf16[256,1536]{1,0:T(8,128)(2,1)S(1)} collective-permute-done((bf16[256,1536]{1,0:T(8,128)(2,1)}, bf16[256,1536]{1,0:T(8,128)(2,1)S(1)}, u32[]{:S(2)}, u32[]{:S(2)}) %collective-permute-start.14) | collective-permute-done | bytes 786464 | tf_op jit(solution)/shard_map/ppermute | solution.py:11
  360.4 4.4 %dynamic_update_slice.13 = bf16[256,1408]{1,0:T(8,128)(2,1)S(1)} dynamic-update-slice(bf16[256,1408]{1,0:T(8,128)(2,1)S(1)} %dynamic_update_slice.12, bf16[256,768]{1,0:T(8,128)(2,1)S(1)} %get-tuple-element.27, s32[]{:T(128)} %constant.64.clone.1, s32[]{:T(128)S(6)} %select_n.85) | dynamic-update-slice | bytes 786436 | tf_op jit(solution)/shard_map/dynamic_update_slice | solution.py:120
  366.0 4.3 %dynamic_update_slice.15 = bf16[256,1408]{1,0:T(8,128)(2,1)S(1)} dynamic-update-slice(bf16[256,1408]{1,0:T(8,128)(2,1)S(1)} %dynamic_update_slice.14, bf16[256,768]{1,0:T(8,128)(2,1)S(1)} %get-tuple-element.26, s32[]{:T(128)} %constant.64.clone.1, s32[]{:T(128)S(6)} %select_n.85) | dynamic-update-slice | bytes 786436 | tf_op jit(solution)/shard_map/dynamic_update_slice | solution.py:120
  (92 shorter events, 36.6 us)
Async XLA Ops:
  7.2 157.9 %all-gather.3.cloned.1.call-start = ((), (), s32[]{:S(2)}) async-start(), calls=%async_computation.2 | async-start | bytes 6291456 | tf_op jit(solution)/shard_map/all_gather | solution.py:68
  8.8 22.2 %collective-permute-start.6 = (bf16[256,1536]{1,0:T(8,128)(2,1)S(1)}, bf16[256,1536]{1,0:T(8,128)(2,1)S(1)}, u32[]{:S(2)}, u32[]{:S(2)}) collective-permute-start(bf16[256,1536]{1,0:T(8,128)(2,1)S(1)} %pad_maximum_fusion.8), channel_id=1, source_target_pairs={{0,2},{2,4},{4,6},{6,8},{8,10},{10,12},{12,14},{14,0},{1,3},{3,5},... | collective-permute-start | bytes 2359304 | tf_op jit(solution)/shard_map/ppermute | solution.py:58
  30.9 31.4 %copy-start.1 = (bf16[256,1536]{1,0:T(8,128)(2,1)}, bf16[256,1536]{1,0:T(8,128)(2,1)S(1)}, u32[]{:S(2)}) copy-start(bf16[256,1536]{1,0:T(8,128)(2,1)S(1)} %collective-permute-done.6) | copy-start | bytes 2359300
  31.0 31.4 %collective-permute-start.7 = (bf16[256,1536]{1,0:T(8,128)(2,1)S(1)}, bf16[256,1536]{1,0:T(8,128)(2,1)}, u32[]{:S(2)}, u32[]{:S(2)}) collective-permute-start(bf16[256,1536]{1,0:T(8,128)(2,1)S(1)} %collective-permute-done.6), channel_id=1, source_target_pairs={{0,2},{2,4},{4,6},{6,8},{8,10},{10,12},{12,14},{14,0},{1,3},{3,5},... | collective-permute-start | bytes 2359304 | tf_op jit(solution)/shard_map/ppermute | solution.py:58
  32.9 25.7 %collective-permute-start.4 = (bf16[8,1024]{0,1:T(8,128)(2,1)S(1)}, bf16[8,1024]{0,1:T(8,128)(2,1)}, u32[]{:S(2)}, u32[]{:S(2)}) collective-permute-start(bf16[8,1024]{0,1:T(8,128)(2,1)S(1)} %get-tuple-element.31), channel_id=1, source_target_pairs={{0,2},{2,4},{4,6},{6,8},{8,10},{10,12},{12,14},{1,3},{3,5},{5,7},{... | collective-permute-start | bytes 49160 | tf_op jit(solution)/shard_map/ppermute | solution.py:17
  36.3 22.2 %collective-permute-start.3 = (bf16[8,1024]{0,1:T(8,128)(2,1)S(1)}, bf16[8,1024]{0,1:T(8,128)(2,1)S(1)}, u32[]{:S(2)}, u32[]{:S(2)}) collective-permute-start(bf16[8,1024]{0,1:T(8,128)(2,1)S(1)} %get-tuple-element.30), channel_id=1, source_target_pairs={{2,0},{4,2},{6,4},{8,6},{10,8},{12,10},{14,12},{3,1},{5,3},{7,5},{... | collective-permute-start | bytes 49160 | tf_op jit(solution)/shard_map/ppermute | solution.py:16
  58.5 0.7 copy-start.4
  61.6 19.8 %collective-permute-start.5 = (bf16[400,1024]{1,0:T(8,128)(2,1)}, bf16[400,1024]{1,0:T(8,128)(2,1)}, u32[]{:S(2)}, u32[]{:S(2)}) collective-permute-start(bf16[400,1024]{1,0:T(8,128)(2,1)} %copy.21), channel_id=1, source_target_pairs={{0,16},{16,0},{1,17},{17,1},{2,18},{18,2},{3,19},{19,3},{4,20},{20... | collective-permute-start | bytes 2457608 | tf_op jit(solution)/shard_map/ppermute | solution.py:11
  62.3 21.5 %collective-permute-start.8 = (bf16[256,1536]{1,0:T(8,128)(2,1)}, bf16[256,1536]{1,0:T(8,128)(2,1)}, u32[]{:S(2)}, u32[]{:S(2)}) collective-permute-start(bf16[256,1536]{1,0:T(8,128)(2,1)} %collective-permute-done.7), channel_id=1, source_target_pairs={{0,2},{2,4},{4,6},{6,8},{8,10},{10,12},{12,14},{14,0},{1,3},{3,5},... | collective-permute-start | bytes 2359304 | tf_op jit(solution)/shard_map/ppermute | solution.py:58
  83.8 20.6 %collective-permute-start.9 = (bf16[256,1536]{1,0:T(8,128)(2,1)}, bf16[256,1536]{1,0:T(8,128)(2,1)}, u32[]{:S(2)}, u32[]{:S(2)}) collective-permute-start(bf16[256,1536]{1,0:T(8,128)(2,1)} %collective-permute-done.8), channel_id=1, source_target_pairs={{0,2},{2,4},{4,6},{6,8},{8,10},{10,12},{12,14},{14,0},{1,3},{3,5},... | collective-permute-start | bytes 2359304 | tf_op jit(solution)/shard_map/ppermute | solution.py:58
  86.3 172.7 %reduce-scatter.3.cloned.1.call-start = ((), (), s32[]{:S(2)}) async-start(), calls=%async_computation.3 | async-start | bytes 4718592 | tf_op jit(solution)/shard_map/reduce_scatter | solution.py:101
  104.4 19.6 %collective-permute-start.10 = (bf16[256,1536]{1,0:T(8,128)(2,1)}, bf16[256,1536]{1,0:T(8,128)(2,1)S(1)}, u32[]{:S(2)}, u32[]{:S(2)}) collective-permute-start(bf16[256,1536]{1,0:T(8,128)(2,1)} %collective-permute-done.9), channel_id=1, source_target_pairs={{0,2},{2,4},{4,6},{6,8},{8,10},{10,12},{12,14},{14,0},{1,3},{3,5},... | collective-permute-start | bytes 2359304 | tf_op jit(solution)/shard_map/ppermute | solution.py:58
  124.1 18.6 %collective-permute-start.11 = (bf16[256,1536]{1,0:T(8,128)(2,1)S(1)}, bf16[256,1536]{1,0:T(8,128)(2,1)S(1)}, u32[]{:S(2)}, u32[]{:S(2)}) collective-permute-start(bf16[256,1536]{1,0:T(8,128)(2,1)S(1)} %collective-permute-done.10), channel_id=1, source_target_pairs={{0,2},{2,4},{4,6},{6,8},{8,10},{10,12},{12,14},{14,0},{1,3},{3,5},... | collective-permute-start | bytes 2359304 | tf_op jit(solution)/shard_map/ppermute | solution.py:58
  142.7 28.5 %collective-permute-start.12 = (bf16[256,1536]{1,0:T(8,128)(2,1)S(1)}, bf16[256,1536]{1,0:T(8,128)(2,1)S(1)}, u32[]{:S(2)}, u32[]{:S(2)}) collective-permute-start(bf16[256,1536]{1,0:T(8,128)(2,1)S(1)} %collective-permute-done.11), channel_id=1, source_target_pairs={{0,2},{2,4},{4,6},{6,8},{8,10},{10,12},{12,14},{14,0},{1,3},{3,5},... | collective-permute-start | bytes 2359304 | tf_op jit(solution)/shard_map/ppermute | solution.py:58
  143.4 13.0 %collective-permute-start.1 = (bf16[8,1408]{1,0:T(8,128)(2,1)S(1)}, bf16[8,1408]{1,0:T(8,128)(2,1)S(1)}, u32[]{:S(2)}, u32[]{:S(2)}) collective-permute-start(bf16[8,1408]{1,0:T(8,128)(2,1)S(1)} %get-tuple-element.25), channel_id=1, source_target_pairs={{0,2},{2,4},{4,6},{6,8},{8,10},{10,12},{12,14},{1,3},{3,5},{5,7},{... | collective-permute-start | bytes 67592 | tf_op jit(solution)/shard_map/ppermute | solution.py:17
  146.8 14.0 %collective-permute-start = (bf16[8,1408]{1,0:T(8,128)(2,1)S(1)}, bf16[8,1408]{1,0:T(8,128)(2,1)S(1)}, u32[]{:S(2)}, u32[]{:S(2)}) collective-permute-start(bf16[8,1408]{1,0:T(8,128)(2,1)S(1)} %get-tuple-element.24), channel_id=1, source_target_pairs={{2,0},{4,2},{6,4},{8,6},{10,8},{12,10},{14,12},{3,1},{5,3},{7,5},{... | collective-permute-start | bytes 67592 | tf_op jit(solution)/shard_map/ppermute | solution.py:16
  163.8 24.5 %collective-permute-start.2 = (bf16[400,768]{1,0:T(8,128)(2,1)}, bf16[400,768]{1,0:T(8,128)(2,1)}, u32[]{:S(2)}, u32[]{:S(2)}) collective-permute-start(bf16[400,768]{1,0:T(8,128)(2,1)} %get-tuple-element.23), channel_id=1, source_target_pairs={{0,16},{16,0},{1,17},{17,1},{2,18},{18,2},{3,19},{19,3},{4,20},{20... | collective-permute-start | bytes 1843208 | tf_op jit(solution)/shard_map/ppermute | solution.py:11
  171.1 3.8 %copy-start.2 = (bf16[256,1536]{1,0:T(8,128)(2,1)S(1)}, bf16[256,1536]{1,0:T(8,128)(2,1)}, u32[]{:S(2)}) copy-start(bf16[256,1536]{1,0:T(8,128)(2,1)} %copy-done.1) | copy-start | bytes 2359300
  175.2 3.9 %copy-start = (bf16[2,400,2048]{2,1,0:T(8,128)(2,1)S(1)}, bf16[2,400,2048]{2,1,0:T(8,128)(2,1)}, u32[]{:S(2)}) copy-start(bf16[2,400,2048]{2,1,0:T(8,128)(2,1)} %copy.23) | copy-start | bytes 9830404
  179.1 5.5 %copy-start.5 = (bf16[4096,1536]{1,0:T(8,128)(2,1)}, bf16[4096,1536]{1,0:T(8,128)(2,1)S(1)}, u32[]{:S(2)}) copy-start(bf16[4096,1536]{1,0:T(8,128)(2,1)S(1)} %constant_dynamic-update-slice_fusion) | copy-start | bytes 37748740
  186.6 1.7 copy-start.3
  209.1 132.1 %reduce-scatter.5.cloned.1.call-start = ((), (), s32[]{:S(2)}) async-start(), calls=%async_computation.4 | async-start | bytes 7077888 | tf_op jit(solution)/shard_map/reduce_scatter | solution.py:97
  260.2 82.2 %collective-permute-start.13 = (bf16[384,1024]{1,0:T(8,128)(2,1)S(1)}, bf16[384,1024]{1,0:T(8,128)(2,1)S(1)}, u32[]{:S(2)}, u32[]{:S(2)}) collective-permute-start(bf16[384,1024]{1,0:T(8,128)(2,1)S(1)} %slice.184), channel_id=1, source_target_pairs={{0,16},{16,0},{1,17},{17,1},{2,18},{18,2},{3,19},{19,3},{4,20},{20... | collective-permute-start | bytes 2359304 | tf_op jit(solution)/shard_map/ppermute | solution.py:11
  341.2 18.7 %collective-permute-start.14 = (bf16[256,1536]{1,0:T(8,128)(2,1)}, bf16[256,1536]{1,0:T(8,128)(2,1)S(1)}, u32[]{:S(2)}, u32[]{:S(2)}) collective-permute-start(bf16[256,1536]{1,0:T(8,128)(2,1)} %reduce-scatter.5.cloned.1.call-done), channel_id=1, source_target_pairs={{0,16},{16,0},{1,17},{17,1},{2,18},{18,2},{3,19},{19,3},{4,20},{20... | collective-permute-start | bytes 2359304 | tf_op jit(solution)/shard_map/ppermute | solution.py:11
Sparse Core Ops, SparseCore 0:
  86.4 15.6 all-gather.2
  209.2 9.0 reduce-scatter.2
  221.9 119.2 reduce-scatter.4
